TPU v7x, 512 devices: a whole 4x4x16 slice. The times are simulated.
512 devices in a mesh: sp: 16 (over z), fs: 4 (over y), tp: 8 (over x, core).
Axes of the slice: x: 4, y: 4, z: 16, core: 2. Of those that a mesh axis runs over, the one named last changes fastest.
Arguments:
- tokens: bfloat16 [4, 4096, 2048], P('fs', 'sp'), may hold values from -6 to 6
- norm_gain: float32 [2048], replicated, may hold values from 0.1 to 1.9
- pool_input: bfloat16 [2048, 2048], P(('sp', 'fs'), 'tp'), may hold values from -0.125 to 0.125
- query_weight: bfloat16 [2048, 2048], P(('sp', 'fs'), 'tp'), may hold values from -20 to 20
- key_weight: bfloat16 [2048, 2048], P(('sp', 'fs'), 'tp'), may hold values from -1 to 1
- value_weight: bfloat16 [2048, 2048], P(('sp', 'fs'), 'tp'), may hold values from -0.125 to 0.125
- pool_map: bfloat16 [8, 256, 256], P('tp'), may hold values from -0.375 to 0.375
- pool_scale: float32 [2048], P('tp'), may hold values from 0.1 to 1.9
- head_gain: float32 [256], replicated, may hold values from 0.1 to 1.9
- diff_lambda: float32 [8], replicated, may hold values from 0.3 to 0.8
- out_pool: bfloat16 [2048, 2048], P('tp', ('sp', 'fs')), may hold values from -0.09375 to 0.09375
- out_heads: bfloat16 [2048, 2048], P('tp', ('sp', 'fs')), may hold values from -0.09375 to 0.09375
Outputs:
- layer_out: bfloat16 [4, 4096, 2048], P('fs', 'sp', 'tp')
All inputs are finite; a program needn't handle non-finite values.
Results may differ from a plain program's by a relative error of at most 0.018.
Values may be sent and summed in bfloat16 or wider, within the bound.
A program may use at most 64 MiB of HBM per device.

v0:
```python
import math

import jax
import jax.numpy as jnp
from jax import lax
from jax.sharding import PartitionSpec as P

HEAD_DIM = 128
GROUP_DIM = 256


THETA = 500000.0
HEAD_SCALE = 0.8
NORM_EPS = 1e-06
HEAD_EPS = 1e-05


def gathered_by_axis(x, axes, dim):
    if not axes:
        return x
    nearer = lax.all_gather(x, axes[-1], axis=dim, tiled=True)
    return gathered_by_axis(nearer, axes[:-1], dim)


def in_one_piece(arrays, axis, dim, along):
    widths = [a.shape[along] for a in arrays]
    both = jnp.concatenate(arrays, axis=along)
    filled = lax.all_gather(both, axis, axis=dim, tiled=True)
    return tuple(jnp.split(filled, [sum(widths[:k]) for k in range(1, len(widths))], axis=along))


def from_behind(value, axis, steps):
    count = lax.axis_size(axis)
    first, last = (max(0, -steps), min(count, count - steps))
    return lax.ppermute(value, axis, [(source, source + steps) for source in range(first, last)])


def split_up(x, dim, size):
    before, after = (x.shape[:dim], x.shape[dim + 1 :])
    return jnp.moveaxis(x.reshape(*before, size, -1, *after), dim, 0)


def sent_and_summed(x, axis, dim):
    size = lax.axis_size(axis)
    pieces = lax.all_to_all(split_up(x, dim, size), axis, 0, 0, tiled=True)
    return jnp.sum(pieces.astype(jnp.float32), axis=0)


def rotate(tensor, positions):
    half = HEAD_DIM // 2
    freqs = 1.0 / THETA ** (jnp.arange(half, dtype=jnp.float32) * 2.0 / HEAD_DIM)
    angles = positions[:, None] * freqs[None, :]
    cosine = jnp.cos(angles)[:, None, None, :]
    sine = jnp.sin(angles)[:, None, None, :]
    floated = tensor.astype(jnp.float32)
    first = floated[..., :half]
    second = floated[..., half:]
    turned = jnp.concatenate([first * cosine - second * sine, second * cosine + first * sine], -1)
    return turned.astype(jnp.bfloat16)


def local(
    tokens,
    norm_gain,
    pool_input,
    query_weight,
    key_weight,
    value_weight,
    pool_map,
    pool_scale,
    head_gain,
    diff_lambda,
    out_pool,
    out_heads,
):
    out_local = jnp.concatenate([out_pool, out_heads], 0)
    out_whole = gathered_by_axis(out_local, ("sp", "fs"), 1)
    row_count = tokens.shape[1]
    floated = tokens[0].astype(jnp.float32)
    normed = (
        floated * lax.rsqrt(jnp.mean(floated * floated, -1, keepdims=True) + NORM_EPS) * norm_gain
    ).astype(jnp.bfloat16)
    fragments = in_one_piece(
        (pool_input, query_weight, key_weight, value_weight), ("sp", "fs"), 0, 1
    )
    projected = tuple(
        (jnp.dot(normed, fragment, preferred_element_type=jnp.float32) for fragment in fragments)
    )
    pool_in, queries, keys_flat, values_flat = [
        product.astype(jnp.bfloat16) for product in projected
    ]
    head_count = values_flat.shape[1] // (2 * HEAD_DIM)
    tp_index = lax.axis_index("tp")
    sp_index = lax.axis_index("sp")
    query_pos = sp_index * row_count + jnp.arange(row_count, dtype=jnp.int32)
    positions = query_pos.astype(jnp.float32)
    queries = rotate(queries.reshape(row_count, head_count, 2, HEAD_DIM), positions)
    keys_flat = rotate(keys_flat.reshape(row_count, head_count, 2, HEAD_DIM), positions).reshape(
        row_count, head_count * 2 * HEAD_DIM
    )
    lambdas = lax.dynamic_slice_in_dim(diff_lambda, tp_index * head_count, head_count, 0)

    def online_step(state, key_rows, value_rows, key_offset):
        largest, summed, accum = state
        width = key_rows.shape[0]
        shaped = key_rows.reshape(width, head_count, 2, HEAD_DIM)
        scores = jnp.einsum(
            "qhcd,khcd->chqk", queries, shaped, preferred_element_type=jnp.float32
        ) * HEAD_DIM ** (-0.5)
        key_pos = key_offset + jnp.arange(width, dtype=jnp.int32)
        scores = jnp.where(query_pos[:, None] >= key_pos[None, :], scores, -jnp.inf)
        newest = jnp.maximum(largest, jnp.max(scores, -1))
        anchor = jnp.where(jnp.isfinite(newest), newest, 0.0)
        rescale = jnp.exp(largest - anchor)
        expons = jnp.exp(scores - anchor[..., None])
        summed = summed * rescale + jnp.sum(expons, -1)
        value_shaped = value_rows.reshape(width, head_count, 2 * HEAD_DIM)
        added = jnp.einsum(
            "chqk,khe->chqe",
            expons.astype(jnp.bfloat16),
            value_shaped,
            preferred_element_type=jnp.float32,
        )
        accum = accum * rescale[..., None] + added
        return (newest, summed, accum)

    start_state = (
        jnp.full((2, head_count, row_count), -jnp.inf, jnp.float32),
        jnp.zeros((2, head_count, row_count), jnp.float32),
        jnp.zeros((2, head_count, row_count, 2 * HEAD_DIM), jnp.float32),
    )
    all_keys, all_values = in_one_piece((keys_flat, values_flat), "sp", 0, 1)
    span = math.gcd(all_keys.shape[0], 1024)
    needed = (sp_index * row_count + row_count + span - 1) // span

    def whole_step(index, state):
        offset = index * span
        return online_step(
            state,
            lax.dynamic_slice_in_dim(all_keys, offset, span, 0),
            lax.dynamic_slice_in_dim(all_values, offset, span, 0),
            offset,
        )

    final_state = lax.fori_loop(0, needed, whole_step, start_state)
    summed_final = final_state[1]
    accum_final = final_state[2]
    heads_raw = (
        accum_final[0] / summed_final[0][..., None]
        - lambdas[:, None, None] * accum_final[1] / summed_final[1][..., None]
    )
    heads_raw = jnp.moveaxis(heads_raw, 0, 1)
    attn = (
        (
            heads_raw
            * lax.rsqrt(jnp.mean(heads_raw * heads_raw, -1, keepdims=True) + HEAD_EPS)
            * head_gain
            * HEAD_SCALE
        )
        .astype(jnp.bfloat16)
        .reshape(row_count, head_count * 2 * HEAD_DIM)
    )
    reach = 15
    rim_rows = from_behind(pool_in[row_count - reach :], "sp", 1)
    extended = jnp.concatenate([rim_rows, pool_in], 0).astype(jnp.float32)
    pair_sums = extended[1:] + extended[:-1]
    quad_sums = pair_sums[2:] + pair_sums[:-2]
    octet_sums = quad_sums[4:] + quad_sums[:-4]
    sixteen_sums = octet_sums[8:] + octet_sums[:-8]
    group_count = pool_in.shape[1] // GROUP_DIM
    stacked = jnp.stack(
        [
            pair_sums[14 : 14 + row_count],
            quad_sums[12 : 12 + row_count],
            octet_sums[8 : 8 + row_count],
            sixteen_sums,
        ],
        0,
    ).reshape(4, row_count, group_count, GROUP_DIM)
    levels = (tp_index * group_count + jnp.arange(group_count, dtype=jnp.int32)) % 4
    picked = jnp.sum(
        jnp.where(
            levels[None, None, :, None] == jnp.arange(4, dtype=jnp.int32)[:, None, None, None],
            stacked,
            0.0,
        ),
        0,
    )
    windows = 2 ** (1 + levels)
    counts = jnp.minimum(query_pos[:, None] + 1, windows[None, :]).astype(jnp.float32)
    window_mean = picked / counts[:, :, None]
    grouped = pool_in.reshape(row_count, group_count, GROUP_DIM).astype(jnp.float32)
    pool_mixed = (window_mean - grouped).astype(jnp.bfloat16)
    pooled = (
        (
            jnp.einsum("tgc,gce->tge", pool_mixed, pool_map, preferred_element_type=jnp.float32)
            * pool_scale.reshape(group_count, GROUP_DIM)
        )
        .astype(jnp.bfloat16)
        .reshape(row_count, group_count * GROUP_DIM)
    )
    branches = jnp.concatenate([pooled, attn], 1)
    partial_value = jnp.dot(branches, out_whole, preferred_element_type=jnp.float32)
    layer_out = sent_and_summed(partial_value.astype(jnp.bfloat16), "tp", 1).astype(jnp.bfloat16)
    return layer_out[None]


def solution(mesh):
    placed = (
        P("fs", "sp", None),
        P(),
        P(("sp", "fs"), "tp"),
        P(("sp", "fs"), "tp"),
        P(("sp", "fs"), "tp"),
        P(("sp", "fs"), "tp"),
        P("tp", None, None),
        P("tp"),
        P(),
        P(),
        P("tp", ("sp", "fs")),
        P("tp", ("sp", "fs")),
    )
    return jax.shard_map(
        local, mesh=mesh, in_specs=placed, out_specs=P("fs", "sp", "tp"), check_vma=False
    )
```

profile of v0, /device:TPU:1, one launch (start us, length us, event | category | flops | bytes accessed | tf_op | source)
XLA Modules:
  0.0 359.1 jit_solution(8147833560225114279)
XLA Ops:
  6.5 0.0 copy-start
  6.5 0.0 all-gather.4.cloned.1.call-start
  6.5 1.4 pad_maximum_fusion.3
  8.0 0.0 all-gather.4.cloned.1.call-update
  8.0 0.0 all-gather.6.cloned.1.call-start
  8.1 1.5 fusion.13
  9.6 0.5 multiply_cosine_fusion
  10.1 0.0 copy-start.1
  10.2 0.0 copy-start.5
  10.2 142.4 %all-gather.4.cloned.1.call-done = bf16[2048,1024]{1,0:T(8,128)(2,1)} async-done(((bf16[32,1024]{1,0:T(8,128)(2,1)}), bf16[2048,1024]{1,0:T(8,128)(2,1)}) %all-gather.4.cloned.1.call-update) | async-done | bytes 4194320 | tf_op jit(solution)/shard_map/all_gather | solution.py:28
  152.5 2.2 convolution_convert_fusion.3
  154.8 0.1 copy.43
  154.9 0.1 copy.44
  155.1 0.0 copy-done.1
  155.1 0.0 copy-done.5
  155.1 1.9 convolution_convert_fusion.1
  157.0 0.1 copy.45
  157.1 0.1 copy.46
  157.3 0.1 subtract_convert_fusion
  157.4 0.1 pad_maximum_fusion.1
  157.5 0.1 copy.35
  157.7 0.0 copy-start.2
  157.7 0.0 copy-start.3
  157.7 0.0 copy-start.7
  157.7 1.9 convolution_convert_fusion.2
  159.6 0.7 pad_maximum_fusion
  160.4 0.0 all-gather.6.cloned.1.call-update
  160.4 0.0 all-gather.8.cloned.1.call-start
  160.4 0.0 copy-done.2
  160.4 0.0 copy-done.3
  160.5 9.8 %all_gather.14 = bf16[512,128]{0,1:T(8,128)(2,1)} all-gather(bf16[512,32]{0,1:T(8,128)(2,1)S(1)} %pad_maximum_fusion.4), channel_id=1, replica_groups=mesh['sp'=16,'fs'=4,'tp'=8] {'fs'}, dimensions={1}, use_global_device_ids=true | all-gather | bytes 163840 | tf_op jit(solution)/shard_map/all_gather | solution.py:21
  170.3 0.0 all-gather.8.cloned.1.call-update
  170.4 0.0 copy-done.7
  170.4 0.6 dynamic_slice.9
  171.0 1.7 convolution_convert_fusion.4
  172.8 3.1 collective-permute-start
  175.9 0.1 pad_maximum_fusion.2
  176.0 0.7 collective-permute-done
  176.7 0.0 copy-start.6
  176.9 0.1 fusion.23
  177.0 0.0 copy-done
  177.0 0.4 copy-done.6
  177.4 0.3 fusion.18
  177.7 71.8 %all-gather.6.cloned.1.call-done = bf16[4096,512]{0,1:T(8,128)(2,1)} async-done(((bf16[256,512]{0,1:T(8,128)(2,1)}), bf16[4096,512]{0,1:T(8,128)(2,1)}) %all-gather.6.cloned.1.call-update) | async-done | bytes 4194320 | tf_op jit(solution)/shard_map/all_gather | solution.py:28
  249.5 3.9 %fusion.45 = (bf16[4096,256]{0,1:T(8,128)(2,1)S(1)}, bf16[4096,256]{0,1:T(8,128)(2,1)}) fusion(bf16[4096,512]{0,1:T(8,128)(2,1)} %all-gather.6.cloned.1.call-done), kind=kLoop, calls=%fused_computation.91 | loop fusion | bytes 8388608 | tf_op jit(solution)/shard_map/split | solution.py:29
  253.5 0.0 copy-start.4
  253.5 2.9 while.15
  253.6 1.1 constant_dynamic-slice_fusion.2
  254.7 0.2 broadcast_compare_fusion.2
  254.9 0.5 fusion.62
  255.5 0.6 fusion.66
  256.1 0.3 fusion.65
  256.5 0.6 fusion.35
  257.1 0.0 copy-done.4
  257.1 0.7 fusion.34
  257.8 62.7 %all-gather.8.cloned.1.call-done = bf16[512,2048]{0,1:T(8,128)(2,1)} async-done(((bf16[512,128]{0,1:T(8,128)(2,1)}), bf16[512,2048]{0,1:T(8,128)(2,1)}) %all-gather.8.cloned.1.call-update) | async-done | bytes 2097168 | tf_op jit(solution)/shard_map/all_gather | solution.py:21
  320.5 2.3 convolution_convert_fusion
  322.8 0.1 copy.49
  322.9 28.9 %all_to_all.5 = bf16[8,256,256]{2,1,0:T(8,128)(2,1)S(1)} all-to-all(bf16[8,256,256]{2,1,0:T(8,128)(2,1)S(1)} %bitcast.134), channel_id=1, replica_groups=mesh['sp'=16,'fs'=4,'tp'=8] {'tp'}, dimensions={0} | all-to-all | bytes 2097152 | tf_op jit(solution)/shard_map/all_to_all | solution.py:45
  351.8 0.8 reduce_sum.53
  (26 shorter events, 0.4 us)
Async XLA Ops:
  6.5 170.5 %copy-start = (bf16[1,256,256]{2,1,0:T(8,128)(2,1)S(1)}, bf16[1,256,256]{2,1,0:T(8,128)(2,1)}, u32[]{:S(2)}) copy-start(bf16[1,256,256]{2,1,0:T(8,128)(2,1)} %param.20) | copy-start | bytes 393220
  6.5 146.0 %all-gather.4.cloned.1.call-start = ((), (), s32[]{:S(2)}) async-start(), calls=%async_computation.1 | async-start | bytes 4259840 | tf_op jit(solution)/shard_map/all_gather | solution.py:28
  8.0 241.5 %all-gather.6.cloned.1.call-start = ((), (), s32[]{:S(2)}) async-start(), calls=%async_computation.2 | async-start | bytes 4456448 | tf_op jit(solution)/shard_map/all_gather | solution.py:28
  10.1 144.9 %copy-start.1 = (bf16[1,256,2048]{2,1,0:T(8,128)(2,1)S(1)}, bf16[1,256,2048]{2,1,0:T(8,128)(2,1)}, u32[]{:S(2)}) copy-start(bf16[1,256,2048]{2,1,0:T(8,128)(2,1)} %param.14) | copy-start | bytes 3145732
  10.2 144.9 %copy-start.5 = (f32[2048]{0:T(1024)S(1)}, f32[2048]{0:T(1024)}, u32[]{:S(2)}) copy-start(f32[2048]{0:T(1024)} %param.15) | copy-start | bytes 24580
  157.7 2.8 copy-start.2
  157.7 2.8 copy-start.3
  157.7 12.7 %copy-start.7 = (f32[8]{0:T(128)S(1)}, f32[8]{0:T(128)}, u32[]{:S(2)}) copy-start(f32[8]{0:T(128)} %param.23) | copy-start | bytes 100
  160.4 160.1 %all-gather.8.cloned.1.call-start = ((), (), s32[]{:S(2)}) async-start(), calls=%async_computation.3 | async-start | bytes 2228224 | tf_op jit(solution)/shard_map/all_gather | solution.py:21
  172.8 3.9 %collective-permute-start = (bf16[15,256]{1,0:T(8,128)(2,1)S(1)}, bf16[15,256]{1,0:T(8,128)(2,1)S(1)}, u32[]{:S(2)}, u32[]{:S(2)}) collective-permute-start(bf16[15,256]{1,0:T(8,128)(2,1)S(1)} %slice.77), channel_id=1, source_target_pairs={{0,32},{32,64},{64,96},{96,128},{128,160},{160,192},{192,224},{224... | collective-permute-start | bytes 23048 | tf_op jit(solution)/shard_map/ppermute | solution.py:35
  176.7 0.7 copy-start.6
  253.5 3.6 copy-start.4
Sparse Core Ops, SparseCore 0:
  10.3 142.2 all-gather.3
  160.5 88.9 all-gather.5
  251.6 68.7 all-gather.7
where the time goes:
time: 360 us; the launch traced here: 359 us
  waiting for transfers between devices  278 us (77%)
  blocking collectives  38.7 us (11%)
  between operations  13.5 us (4%)
  matrix products  11.6 us (3%)
  other arithmetic  7.6 us (2%)
  local copies, waits for them, and re-layouts  6.85 us (2%)
    all_gather x2, waiting for transfers between devices, in_one_piece(): filled = lax.all_gather(both, axis, axis=dim, tiled=True)  214 us
    all_gather x1, waiting for transfers between devices, gathered_by_axis(): nearer = lax.all_gather(x, axes[-1], axis=dim, tiled=True)  62.7 us
    all_to_all x1, blocking collectives, sent_and_summed(): pieces = lax.all_to_all(split_up(x, dim, size), axis, 0, 0, tiled=True)  28.9 us
    all_gather x1, blocking collectives, gathered_by_axis(): nearer = lax.all_gather(x, axes[-1], axis=dim, tiled=True)  9.85 us
    dot_general x4, matrix products, local(): jnp.dot(normed, fragment, preferred_element_type=jnp.float32)  7.76 us
  transfers between devices with their start and end apart: 4, of which 4 were waited for; matrix products, arithmetic and copies ran while one was open for 4% of the time, Pallas kernels for 0%

commit v1 on v0

v1 whole, which is shorter than its diff:
```python
import functools

import numpy as np
import jax
import jax.numpy as jnp
from jax import lax
from jax.experimental import pallas as pl
from jax.experimental.pallas import tpu as pltpu
from jax.sharding import PartitionSpec as P

HEAD_DIM = 128
THETA = 500000.0
HEAD_SCALE = 0.8
NORM_EPS = 1e-06
HEAD_EPS = 1e-05
NEG = -1e30
F32 = jnp.float32
BF16 = jnp.bfloat16
MESH = pl.DeviceIdType.MESH
LOG2E = 1.4426950408889634


def rope_tables(rows, blocks):
    half = HEAD_DIM // 2
    freqs = 1.0 / THETA ** (np.arange(half, dtype=np.float64) * 2.0 / HEAD_DIM)
    tables = []
    for offsets in (np.arange(rows), np.arange(blocks) * rows):
        angles = offsets[:, None] * freqs[None, :]
        cosine, sine = np.cos(angles), np.sin(angles)
        tables.append(np.concatenate([cosine, cosine], 1).astype(np.float32))
        tables.append(np.concatenate([sine, sine], 1).astype(np.float32))
    return tables


def remote(src, dst, send, recv, **where):
    return pltpu.make_async_remote_copy(
        src_ref=src, dst_ref=dst, send_sem=send, recv_sem=recv, device_id=where, device_id_type=MESH
    )


def nt_dot(a, b):
    return lax.dot_general(a, b, (((1,), (1,)), ((), ())), preferred_element_type=F32)


def kernel(
    nz, ny, nt,
    tok, gain, pin, qw, kw, vw, pmap, pscale, hgain, lam, opool, ohead,
    rowcos, rowsin, blkcos, blksin,
    out,
    nrm, wkv, wqp, wo, kv, qbuf, poolbuf, rim, bra, part, rs,
    m_ref, l_ref, acc,
    loc_sem, zsend, zrecv, ysend, yleft, yright, yopp, ksend, krecv, rimsem, rssend, rsrecv,
):
    z = lax.axis_index("sp")
    y = lax.axis_index("fs")
    t = lax.axis_index("tp")
    zr1 = lax.rem(z + 1, nz)
    zl1 = lax.rem(z + nz - 1, nz)
    yr1 = lax.rem(y + 1, ny)
    yl1 = lax.rem(y + ny - 1, ny)
    rows = tok.shape[0]
    far = nz // 2
    groups = (wkv, wqp, wo)

    def slot(zz, yy):
        return pl.ds(pl.multiple_of(zz * 128 + yy * 32, 32), 32)

    own = slot(z, y)
    loads = [
        pltpu.make_async_copy(kw, wkv.at[own, 0:256], loc_sem.at[0]),
        pltpu.make_async_copy(vw, wkv.at[own, 256:512], loc_sem.at[1]),
        pltpu.make_async_copy(pin, wqp.at[own, 0:256], loc_sem.at[2]),
        pltpu.make_async_copy(qw, wqp.at[own, 256:512], loc_sem.at[3]),
    ]
    for load in loads:
        load.start()

    barrier = pltpu.get_barrier_semaphore()
    for where in ({"sp": zr1}, {"sp": zl1}, {"fs": yr1}, {"fs": yl1}):
        pl.semaphore_signal(barrier, inc=1, device_id=where, device_id_type=MESH)
    for k in range(1, nt):
        pl.semaphore_signal(
            barrier, inc=1, device_id={"tp": lax.rem(t + k, nt)}, device_id_type=MESH
        )
    for load in loads:
        load.wait()
    pl.semaphore_wait(barrier, 4 + nt - 1)

    def zslot(s, way):
        return lax.rem(z + nz - s, nz) if way == 0 else lax.rem(z + s, nz)

    def zcopy(g, way, s):
        at = slot(zslot(s, way), y)
        peer = zr1 if way == 0 else zl1
        return remote(
            groups[g].at[at], groups[g].at[at], zsend.at[g, way, s], zrecv.at[g, way, s], sp=peer
        )

    def zwait(g, way, s):
        at = slot(zslot(s, way), y)
        remote(
            groups[g].at[at], groups[g].at[at], zsend.at[g, way, s - 1], zrecv.at[g, way, s - 1], sp=zl1
        ).wait_recv()

    last = (far, nz - far - 1)

    def index_of(s, way):
        return 0 if s == 0 else 2 * s - 1 + way

    def steps_at(s):
        return [(s, way) for way in (0, 1) if s <= last[way] and not (s == 0 and way == 1)]

    def ysend_slots(g, s, way):
        buf = groups[g]
        at = slot(zslot(s, way), y)
        i = index_of(s, way)
        remote(buf.at[at], buf.at[at], ysend.at[g], yleft.at[g, i], fs=yr1).start()
        remote(buf.at[at], buf.at[at], ysend.at[g], yright.at[g, i], fs=yl1).start()

    def yrelay(g, s, way):
        buf = groups[g]
        zz = zslot(s, way)
        i = index_of(s, way)
        at = slot(zz, yl1)
        remote(buf.at[at], buf.at[at], ysend.at[g], yleft.at[g, i], fs=yr1).wait_recv()
        half = pl.ds(pl.multiple_of(zz * 128 + yl1 * 32, 16), 16)
        remote(buf.at[half], buf.at[half], ysend.at[g], yopp.at[g, 0], fs=yr1).start()
        at = slot(zz, yr1)
        remote(buf.at[at], buf.at[at], ysend.at[g], yright.at[g, i], fs=yl1).wait_recv()
        half = pl.ds(pl.multiple_of(zz * 128 + yr1 * 32 + 16, 16), 16)
        remote(buf.at[half], buf.at[half], ysend.at[g], yopp.at[g, 1], fs=yl1).start()

    def yfinish(g):
        buf = groups[g]
        for way in (0, 1):
            quarter = buf.at[pl.ds(0, nz * 16)]
            remote(quarter, quarter, ysend.at[g], yopp.at[g, way], fs=yr1).wait_recv()

    for g in (0, 1):
        for way in (0, 1):
            zcopy(g, way, 0).start()
    ysend_slots(0, 0, 0)

    eye = (
        lax.broadcasted_iota(jnp.int32, (256, 256), 0) == lax.broadcasted_iota(jnp.int32, (256, 256), 1)
    ).astype(BF16)
    for which, src in ((0, opool), (1, ohead)):
        turned = lax.dot_general(
            src[...], eye, (((0,), (0,)), ((), ())), preferred_element_type=F32
        )
        wo[own, which * 256 : which * 256 + 256] = turned.astype(BF16)

    def norm_rows(i, carry):
        at = pl.ds(pl.multiple_of(i * 32, 32), 32)
        x = tok[at, :].astype(F32)
        scale = lax.rsqrt(jnp.mean(x * x, -1, keepdims=True) + NORM_EPS)
        nrm[at, :] = (x * scale * gain[...]).astype(BF16)
        return carry

    lax.fori_loop(0, rows // 32, norm_rows, 0)
    for way in (0, 1):
        zcopy(2, way, 0).start()

    for s in range(1, far + 1):
        for g in range(3):
            for step, way in steps_at(s):
                zwait(g, way, step)
                if step < last[way]:
                    zcopy(g, way, step).start()
                if g == 0:
                    ysend_slots(0, step, way)
        for step, way in steps_at(s - 1):
            yrelay(0, step, way)
    for step, way in steps_at(far):
        yrelay(0, step, way)
    yfinish(0)

    cosine = rowcos[...] * blkcos[pl.ds(z, 1), :] - rowsin[...] * blksin[pl.ds(z, 1), :]
    sine = rowsin[...] * blkcos[pl.ds(z, 1), :] + rowcos[...] * blksin[pl.ds(z, 1), :]
    first = lax.broadcasted_iota(jnp.int32, sine.shape, 1) < HEAD_DIM // 2
    signed = jnp.where(first, -sine, sine)

    def rotated(x):
        x = x.astype(BF16).astype(F32)
        return (x * cosine + pltpu.roll(x, HEAD_DIM // 2, 1) * signed).astype(BF16)

    home = pl.ds(pl.multiple_of(z * rows, rows), rows)
    product = jnp.dot(nrm[...], wkv[:, 0:256], preferred_element_type=F32)
    kv[home, 0:128] = rotated(product[:, 0:128])
    kv[home, 128:256] = rotated(product[:, 128:256])
    kv[home, 256:512] = jnp.dot(nrm[...], wkv[:, 256:512], preferred_element_type=F32).astype(BF16)

    halfrows = rows // 2

    def kslot(s, way, half):
        zz = lax.rem(z + nz - s, nz) if way == 0 else lax.rem(z + s, nz)
        return pl.ds(pl.multiple_of(zz * rows + half * halfrows, halfrows), halfrows)

    def kcopy(s, way, half):
        at = kslot(s, way, half)
        return remote(
            kv.at[at], kv.at[at], ksend.at[way, s, half], krecv.at[way, s, half],
            sp=zr1 if way == 0 else zl1,
        )

    def kwait(s, way, half):
        at = kslot(s, way, half)
        remote(
            kv.at[at], kv.at[at], ksend.at[way, s - 1, half], krecv.at[way, s - 1, half], sp=zl1
        ).wait_recv()

    for half in (0, 1):
        for way in (0, 1):
            kcopy(0, way, half).start()

    order = [pair for s in range(far + 1) for pair in steps_at(s)]
    for step, way in order:
        ysend_slots(1, step, way)

    def ring(s):
        for half in (0, 1):
            for way in (0, 1):
                if s <= last[way]:
                    kwait(s, way, half)
                    if s < last[way]:
                        kcopy(s, way, half).start()

    for s in (1, 2):
        ring(s)
        for step, way in order[(s - 1) * 8 : s * 8]:
            yrelay(1, step, way)
    for step, way in order:
        ysend_slots(2, step, way)
    ring(3)
    yfinish(1)

    product = jnp.dot(nrm[...], wqp[:, 256:512], preferred_element_type=F32)
    qbuf[:, 0:128] = rotated(product[:, 0:128])
    qbuf[:, 128:256] = rotated(product[:, 128:256])
    poolbuf[...] = jnp.dot(nrm[...], wqp[:, 0:256], preferred_element_type=F32).astype(BF16)
    rimcopy = remote(
        poolbuf.at[pl.ds(rows - 16, 16)], rim, rimsem.at[0], rimsem.at[1], sp=zr1
    )
    rimcopy.start()

    score_scale = HEAD_DIM ** (-0.5) * LOG2E

    def scores_of(j, m):
        at = pl.ds(pl.multiple_of(j * rows, rows), rows)
        cols = pl.ds(m * HEAD_DIM, HEAD_DIM)
        return nt_dot(qbuf[:, cols], kv[at, cols]) * score_scale

    def values_of(j):
        return kv[pl.ds(pl.multiple_of(j * rows, rows), rows), 256:512]

    for m in (0, 1):
        s0 = scores_of(z, m)
        above = lax.broadcasted_iota(jnp.int32, s0.shape, 1) > lax.broadcasted_iota(jnp.int32, s0.shape, 0)
        s0 = jnp.where(above, -jnp.inf, s0)
        top = jnp.max(s0, -1, keepdims=True)
        p = jnp.exp2(s0 - top)
        m_ref[m] = top
        l_ref[m] = jnp.sum(p, -1, keepdims=True)
        acc[m] = jnp.dot(p.astype(BF16), values_of(z), preferred_element_type=F32)

    def attend(j):
        for m in (0, 1):
            s0 = scores_of(j, m)
            old = m_ref[m]
            top = jnp.maximum(old, jnp.max(s0, -1, keepdims=True))
            p = jnp.exp2(s0 - top)
            shrink = jnp.exp2(old - top)
            m_ref[m] = top
            l_ref[m] = l_ref[m] * shrink + jnp.sum(p, -1, keepdims=True)
            acc[m] = acc[m] * shrink + jnp.dot(
                p.astype(BF16), values_of(j), preferred_element_type=F32
            )

    def attend_step(s):
        def one(way, carry):
            j = jnp.where(way == 0, z - s, z + s - nz)

            @pl.when(jnp.logical_and(j >= 0, s + way <= far))
            def _():
                attend(j)

            return carry

        lax.fori_loop(0, 2, one, 0)

    def backlog(s, carry):
        attend_step(s)
        return carry

    lax.fori_loop(1, 4, backlog, 0)

    for s in range(4, far + 1):
        ring(s)
        if s in (5, 6):
            for step, way in order[(s - 5) * 8 : (s - 4) * 8]:
                yrelay(2, step, way)
        if s == 4:
            rimcopy.wait_recv()
            level = lax.rem(t, 4)
            inner = poolbuf[...].astype(F32)
            before = jnp.where(z == 0, 0.0, rim[...].astype(F32))
            grown = jnp.concatenate([before, inner], 0)
            picked = jnp.zeros_like(grown)
            for power in range(4):
                grown = grown + pltpu.roll(grown, 1 << power, 0)
                picked = jnp.where(level == power, grown, picked)
            place = z * rows + lax.broadcasted_iota(jnp.int32, (rows, 1), 0)
            window = jnp.left_shift(2, level)
            count = jnp.minimum(place + 1, window).astype(F32)
            mixed = (picked[16:, :] / count - inner).astype(BF16)
            pooled = jnp.dot(mixed, pmap[0], preferred_element_type=F32) * pscale[...]
            bra[:, 0:256] = pooled.astype(BF16)
        attend_step(s)

    yfinish(2)
    heads = acc[0] / l_ref[0] - lam[t] * (acc[1] / l_ref[1])
    scale = lax.rsqrt(jnp.mean(heads * heads, -1, keepdims=True) + HEAD_EPS)
    bra[:, 256:512] = (heads * scale * hgain[...] * HEAD_SCALE).astype(BF16)

    def partial_of(peer):
        at = pl.ds(pl.multiple_of(peer * 256, 256), 256)
        return nt_dot(bra[...], wo[at, :]).astype(BF16)

    def rcopy(k):
        peer = lax.rem(t + k, nt)
        return remote(part.at[k], rs.at[k], rssend.at[k], rsrecv.at[k], tp=peer)

    def emit(i, carry):
        k = i + 1
        part[k] = partial_of(lax.rem(t + k, nt))
        rcopy(k).start()
        return carry

    lax.fori_loop(0, nt - 1, emit, 0)
    total = partial_of(t).astype(F32)
    for k in range(1, nt):
        rcopy(k).wait_recv()
        total = total + rs[k].astype(F32)
    out[...] = total.astype(BF16)

    for g in range(3):
        for way in (0, 1):
            for s in range(last[way]):
                zcopy(g, way, s).wait_send()
        whole = groups[g].at[pl.ds(0, nz * 96)]
        remote(whole, whole, ysend.at[g], yopp.at[g, 0], fs=yr1).wait_send()
    for way in (0, 1):
        for s in range(last[way]):
            for half in (0, 1):
                kcopy(s, way, half).wait_send()
    rimcopy.wait_send()
    for k in range(1, nt):
        rcopy(k).wait_send()


def local(nz, ny, nt, tokens, norm_gain, pool_input, query_weight, key_weight, value_weight,
          pool_map, pool_scale, head_gain, diff_lambda, out_pool, out_heads):
    rows = tokens.shape[1]
    tables = [jnp.asarray(table) for table in rope_tables(rows, nz)]
    vmem = pl.BlockSpec(memory_space=pltpu.VMEM)
    anywhere = pl.BlockSpec(memory_space=pl.ANY)
    smem = pl.BlockSpec(memory_space=pltpu.SMEM)
    dma = pltpu.SemaphoreType.DMA
    far = nz // 2
    result = pl.pallas_call(
        functools.partial(kernel, nz, ny, nt),
        out_shape=jax.ShapeDtypeStruct((rows, 256), BF16),
        in_specs=[vmem, vmem, anywhere, anywhere, anywhere, anywhere, vmem, vmem, vmem, smem, vmem, vmem]
        + [vmem] * 4,
        out_specs=vmem,
        scratch_shapes=[
            pltpu.VMEM((rows, 2048), BF16),
            pltpu.VMEM((2048, 512), BF16),
            pltpu.VMEM((2048, 512), BF16),
            pltpu.VMEM((2048, 512), BF16),
            pltpu.VMEM((nz * rows, 512), BF16),
            pltpu.VMEM((rows, 256), BF16),
            pltpu.VMEM((rows, 256), BF16),
            pltpu.VMEM((16, 256), BF16),
            pltpu.VMEM((rows, 512), BF16),
            pltpu.VMEM((nt, rows, 256), BF16),
            pltpu.VMEM((nt, rows, 256), BF16),
            pltpu.VMEM((2, rows, 1), F32),
            pltpu.VMEM((2, rows, 1), F32),
            pltpu.VMEM((2, rows, 256), F32),
            dma((4,)),
            dma((3, 2, far)),
            dma((3, 2, far)),
            dma((3,)),
            dma((3, nz)),
            dma((3, nz)),
            dma((3, 2)),
            dma((2, far, 2)),
            dma((2, far, 2)),
            dma((2,)),
            dma((nt,)),
            dma((nt,)),
        ],
        compiler_params=pltpu.CompilerParams(
            collective_id=0, has_side_effects=True, vmem_limit_bytes=60 * 1024 * 1024
        ),
        name="layer",
    )(
        tokens[0], norm_gain.reshape(1, -1), pool_input, query_weight, key_weight, value_weight,
        pool_map, pool_scale.reshape(1, -1), head_gain.reshape(1, -1), diff_lambda, out_pool, out_heads,
        *tables,
    )
    return result[None]


def solution(mesh):
    placed = (
        P("fs", "sp", None),
        P(),
        P(("sp", "fs"), "tp"),
        P(("sp", "fs"), "tp"),
        P(("sp", "fs"), "tp"),
        P(("sp", "fs"), "tp"),
        P("tp", None, None),
        P("tp"),
        P(),
        P(),
        P("tp", ("sp", "fs")),
        P("tp", ("sp", "fs")),
    )
    sizes = (mesh.shape["sp"], mesh.shape["fs"], mesh.shape["tp"])
    return jax.shard_map(
        functools.partial(local, *sizes), mesh=mesh, in_specs=placed,
        out_specs=P("fs", "sp", "tp"), check_vma=False,
    )
```

time: 360 us -> 113 us (0.31)
  waiting for transfers between devices: 278 us -> 0 us
  Pallas kernels: 0 us -> 109 us
  blocking collectives: 38.7 us -> 0 us
  between operations: 13.5 us -> 0.01 us
  matrix products: 11.6 us -> 0 us
  other arithmetic: 7.6 us -> 0 us
    all_gather x3 -> x0, waiting for transfers between devices: 277 us -> none  [the longest x2 214 us: in_one_piece(): filled = lax.all_gather(both, axis, axis=dim, tiled=True)]
    pallas_call x0 -> x1, Pallas kernels: none -> 109 us  [local(): pl.pallas_call(functools.partial(kernel, nz, ny, nt), out_shape=jax.Shape...]
    all_to_all x1 -> x0, blocking collectives: 28.9 us -> none  [sent_and_summed(): pieces = lax.all_to_all(split_up(x, dim, size), axis, 0, 0, tiled=True)]
    dot_general x8 -> x0, matrix products: 11.6 us -> none  [the longest x4 7.76 us: local(): jnp.dot(normed, fragment, preferred_element_type=jnp.float32)]
    all_gather x1 -> x0, blocking collectives: 9.85 us -> none  [gathered_by_axis(): nearer = lax.all_gather(x, axes[-1], axis=dim, tiled=True)]
    split x1 -> x0, local copies, waits for them, and re-layouts: 3.93 us -> none  [in_one_piece(): jnp.split(filled, [sum(widths[:k]) for k in range(1, len(widths))], axis=...]
  transfers between devices with their start and end apart: 4 -> 0, of which waited for: 4 -> 0; matrix products, arithmetic and copies ran while one was open for 4% -> 0% of each run, Pallas kernels for 0% -> 0%
where the time goes in v1:
time: 113 us
  Pallas kernels  109 us (96%)
  local copies, waits for them, and re-layouts  3.77 us (3%)
    pallas_call x1, Pallas kernels, local(): pl.pallas_call(functools.partial(kernel, nz, ny, nt), out_shape=jax.Shape...  109 us
    unnamed x5, local copies, waits for them, and re-layouts  3.77 us

profile of v1, /device:TPU:1, one launch (start us, length us, event | category | flops | bytes accessed | tf_op | source)
XLA Modules:
  0.0 112.7 jit_solution(12387890554888870818)
XLA Ops:
  0.0 0.0 copy-start
  0.0 1.5 %copy.17.opool = bf16[256,32]{1,0:T(8,128)(2,1)} copy(bf16[256,32]{0,1:T(8,128)(2,1)} %param.26) | data formatting | bytes 32768 | tf_op args[10]
  1.5 0.0 copy-done
  1.5 0.7 copy.18.ohead
  2.2 108.9 %layer.1 = bf16[256,256]{1,0:T(8,128)(2,1)} custom-call(bf16[256,2048]{1,0:T(8,128)(2,1)} %bitcast.5, f32[1,2048]{1,0:T(1,128)} %bitcast.7, bf16[32,256]{1,0:T(8,128)(2,1)} %pin.1, bf16[32,256]{1,0:T(8,128)(2,1)} %qw.1, bf16[32,256]{1,0:T(8,128)(2,1)} %kw.1, bf16[32,256]{1,0:T(8,128)(2,1)} %vw.1, bf16[1,256,256]{2,1,0:T(8,128)(2,1)} %pmap.1, ...), custom_call_target="tpu_custom_call" | custom-call | tf_op jit(solution)/shard_map/layer/pallas_call | solution.py:370
  111.1 1.6 %copy.20 = bf16[1,256,256]{2,1,0:T(8,128)(2,1)} copy(bf16[1,256,256]{2,1,0:T(8,128)(2,1)} %bitcast.6) | data formatting | bytes 262144
Async XLA Ops:
  0.0 1.5 %copy-start = (bf16[256,32]{0,1:T(8,128)(2,1)S(1)}, bf16[256,32]{0,1:T(8,128)(2,1)}, u32[]{:S(2)}) copy-start(bf16[256,32]{0,1:T(8,128)(2,1)} %param.27) | copy-start | bytes 49156

commit v2 on v1

--- a/solution.py
+++ b/solution.py
@@ -44,12 +44,13 @@
 
 def kernel(
     nz, ny, nt,
-    tok, gain, pin, qw, kw, vw, pmap, pscale, hgain, lam, opool, ohead,
-    rowcos, rowsin, blkcos, blksin,
+    tok_in, gain_in, pin, qw, kw, vw, pmap_in, pscale_in, hgain_in, lam_in, opool, ohead,
+    rowcos_in, rowsin_in, blkcos_in, blksin_in,
     out,
+    tok, gain, pmap, pscale, hgain, lam, rowcos, rowsin, blkcos, blksin,
     nrm, wkv, wqp, wo, kv, qbuf, poolbuf, rim, bra, part, rs,
-    m_ref, l_ref, acc,
-    loc_sem, zsend, zrecv, ysend, yleft, yright, yopp, ksend, krecv, rimsem, rssend, rsrecv,
+    m_ref, l_ref, acc, mate, opp_in, side_in, opp_out,
+    loc_sem, zsend, zrecv, ysend, yleft, yright, yopp, ksend, krecv, rimsem, dsend, drecv, matesend, materecv, rssend, rsrecv,
 ):
     z = lax.axis_index("sp")
     y = lax.axis_index("fs")
@@ -58,6 +59,9 @@
     zl1 = lax.rem(z + nz - 1, nz)
     yr1 = lax.rem(y + 1, ny)
     yl1 = lax.rem(y + ny - 1, ny)
+    y2 = lax.rem(y + 2, ny)
+    zr2 = lax.rem(z + 2, nz)
+    zl2 = lax.rem(z + nz - 2, nz)
     rows = tok.shape[0]
     far = nz // 2
     groups = (wkv, wqp, wo)
@@ -67,33 +71,55 @@
 
     own = slot(z, y)
     loads = [
-        pltpu.make_async_copy(kw, wkv.at[own, 0:256], loc_sem.at[0]),
-        pltpu.make_async_copy(vw, wkv.at[own, 256:512], loc_sem.at[1]),
-        pltpu.make_async_copy(pin, wqp.at[own, 0:256], loc_sem.at[2]),
-        pltpu.make_async_copy(qw, wqp.at[own, 256:512], loc_sem.at[3]),
+        pltpu.make_async_copy(src, dst, loc_sem.at[i])
+        for i, (src, dst) in enumerate((
+            (kw, wkv.at[own, 0:256]),
+            (vw, wkv.at[own, 256:512]),
+            (pin, wqp.at[own, 0:256]),
+            (qw, wqp.at[own, 256:512]),
+            (opool, wo.at[own, 0:256]),
+            (ohead, wo.at[own, 256:512]),
+            (tok_in, tok),
+            (gain_in, gain),
+            (pmap_in, pmap),
+            (pscale_in, pscale),
+            (hgain_in, hgain),
+            (lam_in, lam),
+            (rowcos_in, rowcos),
+            (rowsin_in, rowsin),
+            (blkcos_in, blkcos),
+            (blksin_in, blksin),
+        ))
     ]
     for load in loads:
         load.start()
 
     barrier = pltpu.get_barrier_semaphore()
-    for where in ({"sp": zr1}, {"sp": zl1}, {"fs": yr1}, {"fs": yl1}):
+    friends = [{"sp": zr1}, {"sp": zl1}, {"sp": zr2}, {"sp": zl2}, {"fs": yr1}, {"fs": yl1}, {"fs": y2}]
+    chip = t // 2
+    side = lax.rem(t, 2)
+    chips = nt // 2
+
+    def device(away):
+        return 2 * lax.rem(chip + away, chips) + side
+
+    xr1, xl1, partner = device(1), device(chips - 1), 2 * chip + 1 - side
+    friends += [{"tp": xr1}, {"tp": xl1}, {"tp": partner}]
+    for where in friends:
         pl.semaphore_signal(barrier, inc=1, device_id=where, device_id_type=MESH)
-    for k in range(1, nt):
-        pl.semaphore_signal(
-            barrier, inc=1, device_id={"tp": lax.rem(t + k, nt)}, device_id_type=MESH
-        )
-    for load in loads:
+    for load in loads[:6]:
         load.wait()
-    pl.semaphore_wait(barrier, 4 + nt - 1)
+    pl.semaphore_wait(barrier, len(friends))
 
     def zslot(s, way):
         return lax.rem(z + nz - s, nz) if way == 0 else lax.rem(z + s, nz)
 
-    def zcopy(g, way, s):
+    def zcopy(g, way, s, stride=1):
         at = slot(zslot(s, way), y)
-        peer = zr1 if way == 0 else zl1
+        peer = ((zr1, zl1), (zr2, zl2))[stride - 1][way]
+        k = s + stride - 1
         return remote(
-            groups[g].at[at], groups[g].at[at], zsend.at[g, way, s], zrecv.at[g, way, s], sp=peer
+            groups[g].at[at], groups[g].at[at], zsend.at[g, way, k], zrecv.at[g, way, k], sp=peer
         )
 
     def zwait(g, way, s):
@@ -130,25 +156,32 @@
         half = pl.ds(pl.multiple_of(zz * 128 + yr1 * 32 + 16, 16), 16)
         remote(buf.at[half], buf.at[half], ysend.at[g], yopp.at[g, 1], fs=yl1).start()
 
+    direct = [pair for s in (far - 1, far) for pair in steps_at(s)]
+
+    def yfar(step, way, i):
+        at = slot(zslot(step, way), y)
+        return remote(wkv.at[at], wkv.at[at], dsend.at[i], drecv.at[i], fs=y2)
+
     def yfinish(g):
         buf = groups[g]
+        count = nz - (len(direct) if g == 0 else 0)
         for way in (0, 1):
-            quarter = buf.at[pl.ds(0, nz * 16)]
-            remote(quarter, quarter, ysend.at[g], yopp.at[g, way], fs=yr1).wait_recv()
-
-    for g in (0, 1):
+            part_rows = buf.at[pl.ds(0, count * 16)]
+            remote(part_rows, part_rows, ysend.at[g], yopp.at[g, way], fs=yr1).wait_recv()
+
+    def lead(way, s):
+        for stride in (2, 1):
+            if s + stride <= last[way]:
+                zcopy(0, way, s, stride).start()
+
+    for way in (0, 1):
+        lead(way, 0)
+    ysend_slots(0, 0, 0)
+    for g in (1, 2):
         for way in (0, 1):
             zcopy(g, way, 0).start()
-    ysend_slots(0, 0, 0)
-
-    eye = (
-        lax.broadcasted_iota(jnp.int32, (256, 256), 0) == lax.broadcasted_iota(jnp.int32, (256, 256), 1)
-    ).astype(BF16)
-    for which, src in ((0, opool), (1, ohead)):
-        turned = lax.dot_general(
-            src[...], eye, (((0,), (0,)), ((), ())), preferred_element_type=F32
-        )
-        wo[own, which * 256 : which * 256 + 256] = turned.astype(BF16)
+    loads[6].wait()
+    loads[7].wait()
 
     def norm_rows(i, carry):
         at = pl.ds(pl.multiple_of(i * 32, 32), 32)
@@ -158,23 +191,39 @@
         return carry
 
     lax.fori_loop(0, rows // 32, norm_rows, 0)
-    for way in (0, 1):
-        zcopy(2, way, 0).start()
-
-    for s in range(1, far + 1):
-        for g in range(3):
+    for load in loads[8:]:
+        load.wait()
+
+    def pass_on(s):
+        for g in (1, 2):
             for step, way in steps_at(s):
                 zwait(g, way, step)
                 if step < last[way]:
                     zcopy(g, way, step).start()
-                if g == 0:
-                    ysend_slots(0, step, way)
-        for step, way in steps_at(s - 1):
+
+    for k in range(1, far // 2 + 1):
+        for way in (0, 1):
+            if 2 * k <= last[way]:
+                zwait(0, way, 2 * k)
+                lead(way, 2 * k)
+        for way in (0, 1):
+            zwait(0, way, 2 * k - 1)
+        fresh = steps_at(2 * k - 1) + steps_at(2 * k)
+        for step, way in fresh:
+            ysend_slots(0, step, way)
+            if (step, way) in direct:
+                yfar(step, way, direct.index((step, way))).start()
+        earlier = [(0, 0)] if k == 1 else steps_at(2 * k - 3) + steps_at(2 * k - 2)
+        for step, way in earlier:
             yrelay(0, step, way)
-    for step, way in steps_at(far):
-        yrelay(0, step, way)
+        pass_on(k)
+    for i, (step, way) in enumerate(direct):
+        at = slot(zslot(step, way), yl1)
+        remote(wkv.at[at], wkv.at[at], ysend.at[0], yleft.at[0, index_of(step, way)], fs=yr1).wait_recv()
+        at = slot(zslot(step, way), yr1)
+        remote(wkv.at[at], wkv.at[at], ysend.at[0], yright.at[0, index_of(step, way)], fs=yl1).wait_recv()
+        yfar(step, way, i).wait_recv()
     yfinish(0)
-
     cosine = rowcos[...] * blkcos[pl.ds(z, 1), :] - rowsin[...] * blksin[pl.ds(z, 1), :]
     sine = rowsin[...] * blkcos[pl.ds(z, 1), :] + rowcos[...] * blksin[pl.ds(z, 1), :]
     first = lax.broadcasted_iota(jnp.int32, sine.shape, 1) < HEAD_DIM // 2
@@ -209,31 +258,41 @@
             kv.at[at], kv.at[at], ksend.at[way, s - 1, half], krecv.at[way, s - 1, half], sp=zl1
         ).wait_recv()
 
+    def halves(s, way):
+        return (0, 1) if s < far else (way,)
+
     for half in (0, 1):
         for way in (0, 1):
             kcopy(0, way, half).start()
 
     order = [pair for s in range(far + 1) for pair in steps_at(s)]
-    for step, way in order:
-        ysend_slots(1, step, way)
+    known = far // 2 + 1
+    pass_on(known)
+    for s in range(known + 1):
+        for step, way in steps_at(s):
+            ysend_slots(1, step, way)
 
     def ring(s):
         for half in (0, 1):
             for way in (0, 1):
-                if s <= last[way]:
+                if half in halves(s, way):
                     kwait(s, way, half)
-                    if s < last[way]:
+                    if s < far and half in halves(s + 1, way):
                         kcopy(s, way, half).start()
 
-    for s in (1, 2):
+    for s in (1, 2, 3):
         ring(s)
-        for step, way in order[(s - 1) * 8 : s * 8]:
+        pass_on(known + s)
+        for step, way in steps_at(known + s):
+            ysend_slots(1, step, way)
+        for step, way in order[(s - 1) * 4 : s * 4]:
             yrelay(1, step, way)
+    ring(4)
+    for step, way in order[12:]:
+        yrelay(1, step, way)
     for step, way in order:
         ysend_slots(2, step, way)
-    ring(3)
     yfinish(1)
-
     product = jnp.dot(nrm[...], wqp[:, 256:512], preferred_element_type=F32)
     qbuf[:, 0:128] = rotated(product[:, 0:128])
     qbuf[:, 128:256] = rotated(product[:, 128:256])
@@ -292,14 +351,14 @@
         attend_step(s)
         return carry
 
-    lax.fori_loop(1, 4, backlog, 0)
-
-    for s in range(4, far + 1):
+    lax.fori_loop(1, 5, backlog, 0)
+
+    for s in range(5, far + 1):
         ring(s)
         if s in (5, 6):
             for step, way in order[(s - 5) * 8 : (s - 4) * 8]:
                 yrelay(2, step, way)
-        if s == 4:
+        if s == 5:
             rimcopy.wait_recv()
             level = lax.rem(t, 4)
             inner = poolbuf[...].astype(F32)
@@ -318,44 +377,84 @@
         attend_step(s)
 
     yfinish(2)
-    heads = acc[0] / l_ref[0] - lam[t] * (acc[1] / l_ref[1])
+    here = lax.broadcasted_iota(jnp.int32, lam.shape, 1) == t
+    weight = jnp.sum(jnp.where(here, lam[...], 0.0), -1, keepdims=True)
+    heads = acc[0] / l_ref[0] - weight * (acc[1] / l_ref[1])
     scale = lax.rsqrt(jnp.mean(heads * heads, -1, keepdims=True) + HEAD_EPS)
     bra[:, 256:512] = (heads * scale * hgain[...] * HEAD_SCALE).astype(BF16)
 
-    def partial_of(peer):
-        at = pl.ds(pl.multiple_of(peer * 256, 256), 256)
-        return nt_dot(bra[...], wo[at, :]).astype(BF16)
-
-    def rcopy(k):
-        peer = lax.rem(t + k, nt)
-        return remote(part.at[k], rs.at[k], rssend.at[k], rsrecv.at[k], tp=peer)
-
-    def emit(i, carry):
-        k = i + 1
-        part[k] = partial_of(lax.rem(t + k, nt))
-        rcopy(k).start()
-        return carry
-
-    lax.fori_loop(0, nt - 1, emit, 0)
-    total = partial_of(t).astype(F32)
-    for k in range(1, nt):
-        rcopy(k).wait_recv()
-        total = total + rs[k].astype(F32)
-    out[...] = total.astype(BF16)
+    def partial_of(away, lane):
+        block = 2 * lax.rem(chip + away, chips) + lane
+        at = pl.ds(pl.multiple_of(block * 256, 256), 256)
+        return nt_dot(bra[...], wo[at, :])
+
+    def to_mate(i):
+        return remote(part.at[i], mate.at[i], matesend.at[i], materecv.at[i], tp=partner)
+
+    sequence = (2, 1, 3, 0)
+
+    for i, away in enumerate(sequence):
+        part[i] = partial_of(away, 1 - side).astype(BF16)
+        to_mate(i).start()
+    half_rows = rows // 2
+    upper, lower = pl.ds(0, half_rows), pl.ds(half_rows, half_rows)
+    own_sum = [partial_of(sequence[0], side)]
+    to_mate(0).wait_recv()
+    opp_out[...] = (own_sum[0] + mate[0].astype(F32)).astype(BF16)
+    far_right = remote(opp_out.at[upper], opp_in.at[0], rssend.at[0], rsrecv.at[0], tp=xr1)
+    far_left = remote(opp_out.at[lower], opp_in.at[1], rssend.at[1], rsrecv.at[1], tp=xl1)
+    far_right.start()
+    far_left.start()
+    right_sum = partial_of(1, side)
+    to_mate(1).wait_recv()
+    right_sum = right_sum + mate[1].astype(F32)
+    rs[0, lower, :] = right_sum[half_rows:].astype(BF16)
+    near = [
+        remote(rs.at[0, lower], side_in.at[0, lower], rssend.at[2], rsrecv.at[2], tp=xr1),
+        remote(rs.at[1, upper], side_in.at[1, upper], rssend.at[3], rsrecv.at[3], tp=xl1),
+        remote(rs.at[0, upper], side_in.at[0, upper], rssend.at[4], rsrecv.at[4], tp=xr1),
+        remote(rs.at[1, lower], side_in.at[1, lower], rssend.at[5], rsrecv.at[5], tp=xl1),
+    ]
+    near[0].start()
+    left_sum = partial_of(3, side)
+    to_mate(2).wait_recv()
+    left_sum = left_sum + mate[2].astype(F32)
+    rs[1, upper, :] = left_sum[:half_rows].astype(BF16)
+    near[1].start()
+    total = partial_of(0, side)
+    to_mate(3).wait_recv()
+    total = total + mate[3].astype(F32)
+    far_right.wait_recv()
+    rs[0, upper, :] = (right_sum[:half_rows] + opp_in[0].astype(F32)).astype(BF16)
+    near[2].start()
+    far_left.wait_recv()
+    rs[1, lower, :] = (left_sum[half_rows:] + opp_in[1].astype(F32)).astype(BF16)
+    near[3].start()
+    for copy in near:
+        copy.wait_recv()
+    out[...] = (total + side_in[0].astype(F32) + side_in[1].astype(F32)).astype(BF16)
 
     for g in range(3):
         for way in (0, 1):
-            for s in range(last[way]):
-                zcopy(g, way, s).wait_send()
-        whole = groups[g].at[pl.ds(0, nz * 96)]
+            for k in range(1, last[way] + 1):
+                at = slot(z, y)
+                remote(
+                    groups[g].at[at], groups[g].at[at], zsend.at[g, way, k - 1], zrecv.at[g, way, k - 1], sp=zl1
+                ).wait_send()
+        count = nz * 96 - (len(direct) * 32 if g == 0 else 0)
+        whole = groups[g].at[pl.ds(0, count)]
         remote(whole, whole, ysend.at[g], yopp.at[g, 0], fs=yr1).wait_send()
+    for i, (step, way) in enumerate(direct):
+        yfar(step, way, i).wait_send()
     for way in (0, 1):
-        for s in range(last[way]):
-            for half in (0, 1):
+        for s in range(far):
+            for half in halves(s + 1, way):
                 kcopy(s, way, half).wait_send()
     rimcopy.wait_send()
-    for k in range(1, nt):
-        rcopy(k).wait_send()
+    for i in range(4):
+        to_mate(i).wait_send()
+    for copy in [far_right, far_left] + near:
+        copy.wait_send()
 
 
 def local(nz, ny, nt, tokens, norm_gain, pool_input, query_weight, key_weight, value_weight,
@@ -364,16 +463,24 @@
     tables = [jnp.asarray(table) for table in rope_tables(rows, nz)]
     vmem = pl.BlockSpec(memory_space=pltpu.VMEM)
     anywhere = pl.BlockSpec(memory_space=pl.ANY)
-    smem = pl.BlockSpec(memory_space=pltpu.SMEM)
     dma = pltpu.SemaphoreType.DMA
     far = nz // 2
     result = pl.pallas_call(
         functools.partial(kernel, nz, ny, nt),
         out_shape=jax.ShapeDtypeStruct((rows, 256), BF16),
-        in_specs=[vmem, vmem, anywhere, anywhere, anywhere, anywhere, vmem, vmem, vmem, smem, vmem, vmem]
-        + [vmem] * 4,
+        in_specs=[anywhere] * 16,
         out_specs=vmem,
         scratch_shapes=[
+            pltpu.VMEM((rows, 2048), BF16),
+            pltpu.VMEM((1, 2048), F32),
+            pltpu.VMEM((1, 256, 256), BF16),
+            pltpu.VMEM((1, 256), F32),
+            pltpu.VMEM((1, 256), F32),
+            pltpu.VMEM((1, nt), F32),
+            pltpu.VMEM((rows, HEAD_DIM), F32),
+            pltpu.VMEM((rows, HEAD_DIM), F32),
+            pltpu.VMEM((nz, HEAD_DIM), F32),
+            pltpu.VMEM((nz, HEAD_DIM), F32),
             pltpu.VMEM((rows, 2048), BF16),
             pltpu.VMEM((2048, 512), BF16),
             pltpu.VMEM((2048, 512), BF16),
@@ -383,12 +490,16 @@
             pltpu.VMEM((rows, 256), BF16),
             pltpu.VMEM((16, 256), BF16),
             pltpu.VMEM((rows, 512), BF16),
-            pltpu.VMEM((nt, rows, 256), BF16),
-            pltpu.VMEM((nt, rows, 256), BF16),
+            pltpu.VMEM((4, rows, 256), BF16),
+            pltpu.VMEM((2, rows, 256), BF16),
             pltpu.VMEM((2, rows, 1), F32),
             pltpu.VMEM((2, rows, 1), F32),
             pltpu.VMEM((2, rows, 256), F32),
-            dma((4,)),
+            pltpu.VMEM((4, rows, 256), BF16),
+            pltpu.VMEM((2, rows // 2, 256), BF16),
+            pltpu.VMEM((2, rows, 256), BF16),
+            pltpu.VMEM((rows, 256), BF16),
+            dma((16,)),
             dma((3, 2, far)),
             dma((3, 2, far)),
             dma((3,)),
@@ -398,8 +509,12 @@
             dma((2, far, 2)),
             dma((2, far, 2)),
             dma((2,)),
-            dma((nt,)),
-            dma((nt,)),
+            dma((3,)),
+            dma((3,)),
+            dma((4,)),
+            dma((4,)),
+            dma((6,)),
+            dma((6,)),
         ],
         compiler_params=pltpu.CompilerParams(
             collective_id=0, has_side_effects=True, vmem_limit_bytes=60 * 1024 * 1024
@@ -407,7 +522,8 @@
         name="layer",
     )(
         tokens[0], norm_gain.reshape(1, -1), pool_input, query_weight, key_weight, value_weight,
-        pool_map, pool_scale.reshape(1, -1), head_gain.reshape(1, -1), diff_lambda, out_pool, out_heads,
+        pool_map, pool_scale.reshape(1, -1), head_gain.reshape(1, -1),
+        diff_lambda.reshape(1, -1), out_pool.T, out_heads.T,
         *tables,
     )
     return result[None]

time: 113 us -> 110 us (0.973)
  local copies, waits for them, and re-layouts: 3.77 us -> 1.57 us
    unnamed x5 -> x1, local copies, waits for them, and re-layouts: 3.77 us -> 1.57 us
    pallas_call x1, Pallas kernels: 109 us -> 108 us  [local(): pl.pallas_call(functools.partial(kernel, nz, ny, nt), out_shape=jax.Shape...]
where the time goes in v2:
time: 110 us; the launch traced here: 109 us
  Pallas kernels  108 us (98%)
  local copies, waits for them, and re-layouts  1.57 us (1%)
    pallas_call x1, Pallas kernels, local(): pl.pallas_call(functools.partial(kernel, nz, ny, nt), out_shape=jax.Shape...  108 us

profile of v2, /device:TPU:1, one launch (start us, length us, event | category | flops | bytes accessed | tf_op | source)
XLA Modules:
  0.0 109.3 jit_solution(10900228052317371830)
XLA Ops:
  0.0 107.7 %layer.1 = bf16[256,256]{1,0:T(8,128)(2,1)} custom-call(bf16[256,2048]{1,0:T(8,128)(2,1)} %bitcast.8, f32[1,2048]{1,0:T(1,128)} %bitcast.12, bf16[32,256]{1,0:T(8,128)(2,1)} %pin.1, bf16[32,256]{1,0:T(8,128)(2,1)} %qw.1, bf16[32,256]{1,0:T(8,128)(2,1)} %kw.1, bf16[32,256]{1,0:T(8,128)(2,1)} %vw.1, bf16[1,256,256]{2,1,0:T(8,128)(2,1)} %pmap_in.1, ...), custom_call_target="tpu_custom_call" | custom-call | tf_op jit(solution)/shard_map/layer/pallas_call | solution.py:468
  107.7 1.6 %copy.18 = bf16[1,256,256]{2,1,0:T(8,128)(2,1)} copy(bf16[1,256,256]{2,1,0:T(8,128)(2,1)} %bitcast.9) | data formatting | bytes 262144

commit v3 on v2

--- a/solution.py
+++ b/solution.py
@@ -217,6 +217,7 @@
         for step, way in earlier:
             yrelay(0, step, way)
         pass_on(k)
+    pass_on(far // 2 + 1)
     for i, (step, way) in enumerate(direct):
         at = slot(zslot(step, way), yl1)
         remote(wkv.at[at], wkv.at[at], ysend.at[0], yleft.at[0, index_of(step, way)], fs=yr1).wait_recv()
@@ -224,6 +225,7 @@
         remote(wkv.at[at], wkv.at[at], ysend.at[0], yright.at[0, index_of(step, way)], fs=yl1).wait_recv()
         yfar(step, way, i).wait_recv()
     yfinish(0)
+    pass_on(far // 2 + 2)
     cosine = rowcos[...] * blkcos[pl.ds(z, 1), :] - rowsin[...] * blksin[pl.ds(z, 1), :]
     sine = rowsin[...] * blkcos[pl.ds(z, 1), :] + rowcos[...] * blksin[pl.ds(z, 1), :]
     first = lax.broadcasted_iota(jnp.int32, sine.shape, 1) < HEAD_DIM // 2
@@ -239,57 +241,54 @@
     kv[home, 128:256] = rotated(product[:, 128:256])
     kv[home, 256:512] = jnp.dot(nrm[...], wkv[:, 256:512], preferred_element_type=F32).astype(BF16)
 
-    halfrows = rows // 2
-
-    def kslot(s, way, half):
-        zz = lax.rem(z + nz - s, nz) if way == 0 else lax.rem(z + s, nz)
-        return pl.ds(pl.multiple_of(zz * rows + half * halfrows, halfrows), halfrows)
-
-    def kcopy(s, way, half):
-        at = kslot(s, way, half)
+    pieces = 4
+    span = rows // pieces
+
+    def kslot(s, way, c):
+        return pl.ds(pl.multiple_of(zslot(s, way) * rows + c * span, span), span)
+
+    def kcopy(s, way, c):
+        at = kslot(s, way, c)
         return remote(
-            kv.at[at], kv.at[at], ksend.at[way, s, half], krecv.at[way, s, half],
+            kv.at[at], kv.at[at], ksend.at[way, s, c], krecv.at[way, s, c],
             sp=zr1 if way == 0 else zl1,
         )
 
-    def kwait(s, way, half):
-        at = kslot(s, way, half)
+    def kwait(s, way, c):
+        at = kslot(s, way, c)
         remote(
-            kv.at[at], kv.at[at], ksend.at[way, s - 1, half], krecv.at[way, s - 1, half], sp=zl1
+            kv.at[at], kv.at[at], ksend.at[way, s - 1, c], krecv.at[way, s - 1, c], sp=zl1
         ).wait_recv()
 
-    def halves(s, way):
-        return (0, 1) if s < far else (way,)
-
-    for half in (0, 1):
-        for way in (0, 1):
-            kcopy(0, way, half).start()
+    def service(s, c):
+        for way in (0, 1):
+            kwait(s, way, c)
+            kept = c < pieces // 2 if way == 0 else c >= pieces // 2
+
+            @pl.when(jnp.logical_or(s < far - 1, kept))
+            def _():
+                kcopy(s, way, c).start()
+
+    for c in range(pieces):
+        for way in (0, 1):
+            kcopy(0, way, c).start()
 
     order = [pair for s in range(far + 1) for pair in steps_at(s)]
-    known = far // 2 + 1
-    pass_on(known)
+    known = far // 2 + 2
     for s in range(known + 1):
         for step, way in steps_at(s):
             ysend_slots(1, step, way)
 
-    def ring(s):
-        for half in (0, 1):
-            for way in (0, 1):
-                if half in halves(s, way):
-                    kwait(s, way, half)
-                    if s < far and half in halves(s + 1, way):
-                        kcopy(s, way, half).start()
-
     for s in (1, 2, 3):
-        ring(s)
-        pass_on(known + s)
-        for step, way in steps_at(known + s):
-            ysend_slots(1, step, way)
-        for step, way in order[(s - 1) * 4 : s * 4]:
-            yrelay(1, step, way)
-    ring(4)
-    for step, way in order[12:]:
-        yrelay(1, step, way)
+        for c in range(pieces):
+            service(s, c)
+            if c == 1 and known + s <= far:
+                pass_on(known + s)
+                for step, way in steps_at(known + s):
+                    ysend_slots(1, step, way)
+            at = (s - 1) * pieces + c
+            for step, way in order[at : at + 1] if at < 8 else order[8 + 2 * (at - 8) : 10 + 2 * (at - 8)]:
+                yrelay(1, step, way)
     for step, way in order:
         ysend_slots(2, step, way)
     yfinish(1)
@@ -312,70 +311,83 @@
     def values_of(j):
         return kv[pl.ds(pl.multiple_of(j * rows, rows), rows), 256:512]
 
-    for m in (0, 1):
-        s0 = scores_of(z, m)
-        above = lax.broadcasted_iota(jnp.int32, s0.shape, 1) > lax.broadcasted_iota(jnp.int32, s0.shape, 0)
-        s0 = jnp.where(above, -jnp.inf, s0)
-        top = jnp.max(s0, -1, keepdims=True)
-        p = jnp.exp2(s0 - top)
-        m_ref[m] = top
-        l_ref[m] = jnp.sum(p, -1, keepdims=True)
-        acc[m] = jnp.dot(p.astype(BF16), values_of(z), preferred_element_type=F32)
-
-    def attend(j):
-        for m in (0, 1):
-            s0 = scores_of(j, m)
-            old = m_ref[m]
-            top = jnp.maximum(old, jnp.max(s0, -1, keepdims=True))
-            p = jnp.exp2(s0 - top)
-            shrink = jnp.exp2(old - top)
-            m_ref[m] = top
-            l_ref[m] = l_ref[m] * shrink + jnp.sum(p, -1, keepdims=True)
-            acc[m] = acc[m] * shrink + jnp.dot(
-                p.astype(BF16), values_of(j), preferred_element_type=F32
-            )
-
-    def attend_step(s):
-        def one(way, carry):
-            j = jnp.where(way == 0, z - s, z + s - nz)
-
-            @pl.when(jnp.logical_and(j >= 0, s + way <= far))
-            def _():
-                attend(j)
-
-            return carry
-
-        lax.fori_loop(0, 2, one, 0)
-
-    def backlog(s, carry):
-        attend_step(s)
+    m_ref[...] = jnp.full(m_ref.shape, NEG, F32)
+    l_ref[...] = jnp.zeros(l_ref.shape, F32)
+    acc[...] = jnp.zeros(acc.shape, F32)
+    above = lax.broadcasted_iota(jnp.int32, (rows, rows), 1) > lax.broadcasted_iota(jnp.int32, (rows, rows), 0)
+
+    def attend(n):
+        step = (n + 1) // 2
+        way = lax.rem(n + 1, 2)
+        j = jnp.where(n == 0, z, jnp.where(way == 0, z - step, z + step - nz))
+
+        @pl.when(j >= 0)
+        def _():
+            for m in (0, 1):
+                s0 = scores_of(j, m)
+                s0 = jnp.where(jnp.logical_and(above, j == z), -jnp.inf, s0)
+                old = m_ref[m]
+                top = jnp.maximum(old, jnp.max(s0, -1, keepdims=True))
+                p = jnp.exp2(s0 - top)
+                shrink = jnp.exp2(old - top)
+                m_ref[m] = top
+                l_ref[m] = l_ref[m] * shrink + jnp.sum(p, -1, keepdims=True)
+                acc[m] = acc[m] * shrink + jnp.dot(
+                    p.astype(BF16), values_of(j), preferred_element_type=F32
+                )
+
+    def zplace(n):
+        step = (n + 1) // 2
+        return jnp.where(lax.rem(n + 1, 2) == 0, lax.rem(z + nz - step, nz), lax.rem(z + step, nz))
+
+    def orelay(n):
+        zz = zplace(n)
+        at = slot(zz, yl1)
+        remote(wo.at[at], wo.at[at], ysend.at[2], yleft.at[2, n], fs=yr1).wait_recv()
+        half = pl.ds(pl.multiple_of(zz * 128 + yl1 * 32, 16), 16)
+        remote(wo.at[half], wo.at[half], ysend.at[2], yopp.at[2, 0], fs=yr1).start()
+        at = slot(zz, yr1)
+        remote(wo.at[at], wo.at[at], ysend.at[2], yright.at[2, n], fs=yl1).wait_recv()
+        half = pl.ds(pl.multiple_of(zz * 128 + yr1 * 32 + 16, 16), 16)
+        remote(wo.at[half], wo.at[half], ysend.at[2], yopp.at[2, 1], fs=yl1).start()
+
+    def busy(i, carry):
+        s, c = 4 + i // pieces, lax.rem(i, pieces)
+        service(s, c)
+        orelay(i)
+
+        @pl.when(c < 3)
+        def _():
+            attend(3 * (s - 4) + c)
+
         return carry
 
-    lax.fori_loop(1, 5, backlog, 0)
-
-    for s in range(5, far + 1):
-        ring(s)
-        if s in (5, 6):
-            for step, way in order[(s - 5) * 8 : (s - 4) * 8]:
-                yrelay(2, step, way)
-        if s == 5:
-            rimcopy.wait_recv()
-            level = lax.rem(t, 4)
-            inner = poolbuf[...].astype(F32)
-            before = jnp.where(z == 0, 0.0, rim[...].astype(F32))
-            grown = jnp.concatenate([before, inner], 0)
-            picked = jnp.zeros_like(grown)
-            for power in range(4):
-                grown = grown + pltpu.roll(grown, 1 << power, 0)
-                picked = jnp.where(level == power, grown, picked)
-            place = z * rows + lax.broadcasted_iota(jnp.int32, (rows, 1), 0)
-            window = jnp.left_shift(2, level)
-            count = jnp.minimum(place + 1, window).astype(F32)
-            mixed = (picked[16:, :] / count - inner).astype(BF16)
-            pooled = jnp.dot(mixed, pmap[0], preferred_element_type=F32) * pscale[...]
-            bra[:, 0:256] = pooled.astype(BF16)
-        attend_step(s)
-
+    lax.fori_loop(0, 4 * pieces, busy, 0)
+    rimcopy.wait_recv()
+    level = lax.rem(t, 4)
+    inner = poolbuf[...].astype(F32)
+    before = jnp.where(z == 0, 0.0, rim[...].astype(F32))
+    grown = jnp.concatenate([before, inner], 0)
+    picked = jnp.zeros_like(grown)
+    for power in range(4):
+        grown = grown + pltpu.roll(grown, 1 << power, 0)
+        picked = jnp.where(level == power, grown, picked)
+    place = z * rows + lax.broadcasted_iota(jnp.int32, (rows, 1), 0)
+    window = jnp.left_shift(2, level)
+    count = jnp.minimum(place + 1, window).astype(F32)
+    mixed = (picked[16:, :] / count - inner).astype(BF16)
+    pooled = jnp.dot(mixed, pmap[0], preferred_element_type=F32) * pscale[...]
+    bra[:, 0:256] = pooled.astype(BF16)
+
+    def late(n, carry):
+        attend(n)
+        return carry
+
+    lax.fori_loop(12, 15, late, 0)
+    for c in range(pieces // 2):
+        kwait(far, 0, c)
+        kwait(far, 1, c + pieces // 2)
+    lax.fori_loop(15, 16, late, 0)
     yfinish(2)
     here = lax.broadcasted_iota(jnp.int32, lam.shape, 1) == t
     weight = jnp.sum(jnp.where(here, lam[...], 0.0), -1, keepdims=True)
@@ -448,8 +460,9 @@
         yfar(step, way, i).wait_send()
     for way in (0, 1):
         for s in range(far):
-            for half in halves(s + 1, way):
-                kcopy(s, way, half).wait_send()
+            for c in range(pieces):
+                if s < far - 1 or c // (pieces // 2) == way:
+                    kcopy(s, way, c).wait_send()
     rimcopy.wait_send()
     for i in range(4):
         to_mate(i).wait_send()
@@ -506,8 +519,8 @@
             dma((3, nz)),
             dma((3, nz)),
             dma((3, 2)),
-            dma((2, far, 2)),
-            dma((2, far, 2)),
+            dma((2, far, 4)),
+            dma((2, far, 4)),
             dma((2,)),
             dma((3,)),
             dma((3,)),

time: 110 us -> 102 us (0.927)
  Pallas kernels: 108 us -> 99.9 us
    pallas_call x1, Pallas kernels: 108 us -> 99.9 us  [local(): pl.pallas_call(functools.partial(kernel, nz, ny, nt), out_shape=jax.Shape...]
where the time goes in v3:
time: 102 us
  Pallas kernels  99.9 us (98%)
  local copies, waits for them, and re-layouts  1.57 us (2%)
    pallas_call x1, Pallas kernels, local(): pl.pallas_call(functools.partial(kernel, nz, ny, nt), out_shape=jax.Shape...  99.9 us

profile of v3, /device:TPU:1, one launch (start us, length us, event | category | flops | bytes accessed | tf_op | source)
XLA Modules:
  0.0 101.5 jit_solution(7104368004158053061)
XLA Ops:
  0.0 99.9 %layer.1 = bf16[256,256]{1,0:T(8,128)(2,1)} custom-call(bf16[256,2048]{1,0:T(8,128)(2,1)} %bitcast.8, f32[1,2048]{1,0:T(1,128)} %bitcast.12, bf16[32,256]{1,0:T(8,128)(2,1)} %pin.1, bf16[32,256]{1,0:T(8,128)(2,1)} %qw.1, bf16[32,256]{1,0:T(8,128)(2,1)} %kw.1, bf16[32,256]{1,0:T(8,128)(2,1)} %vw.1, bf16[1,256,256]{2,1,0:T(8,128)(2,1)} %pmap_in.1, ...), custom_call_target="tpu_custom_call" | custom-call | tf_op jit(solution)/shard_map/layer/pallas_call | solution.py:481
  99.9 1.6 %copy.18 = bf16[1,256,256]{2,1,0:T(8,128)(2,1)} copy(bf16[1,256,256]{2,1,0:T(8,128)(2,1)} %bitcast.9) | data formatting | bytes 262144
